TPU v7x, 32 devices: a whole 2x2x4 slice. The times are simulated.
32 devices in a mesh: sp: 8 (over z, y), tp: 4 (over x, core).
Axes of the slice: x: 2, y: 2, z: 4, core: 2. Of those that a mesh axis runs over, the one named last changes fastest.
Arguments:
- residual_in: bfloat16 [6144, 2048], P('sp', 'tp'), may hold values from -11 to 11
- queries: bfloat16 [6144, 1024], P('sp', 'tp'), may hold values from -6 to 6
- keys: bfloat16 [6144, 256], P('sp'), may hold values from -6 to 6
- values: bfloat16 [6144, 256], P('sp'), may hold values from -6 to 6
- query_gain: float32 [128], replicated, may hold values from 1.5 to 5
- key_norm_gain: float32 [128], replicated, may hold values from 1.5 to 5
- out_weight: bfloat16 [1024, 2048], P('tp'), may hold values from -0.1875 to 0.1875
- mlp_gain: float32 [2048], replicated, may hold values from 0.1 to 1.9
- gate_weight: bfloat16 [2048, 5632], P('sp', 'tp'), may hold values from -0.125 to 0.125
- up_weight: bfloat16 [2048, 5632], P('sp', 'tp'), may hold values from -0.125 to 0.125
- down_weight: bfloat16 [5632, 2048], P('tp', 'sp'), may hold values from -0.15625 to 0.15625
Outputs:
- layer_out: bfloat16 [6144, 2048], P('sp', 'tp')
All inputs are finite; a program needn't handle non-finite values.
Results may differ from a plain program's by a relative error of at most 0.012.
The roundings to bfloat16 on the way count: a program that leaves them out, or rounds other values in their place, can miss the bound.
Values may be sent and summed in bfloat16 or wider, within the bound.
No kernel may reach another device: no remote copies, remote signals or barrier semaphores. Data moves between devices by JAX's collectives and lax.ppermute only.
A program may use at most 64 MiB of HBM per device.

v0:
```python
import jax
import jax.numpy as jnp
from jax import lax
from jax.sharding import PartitionSpec as P

D = 2048
HEAD_SIZE = 128
QUERY_HEADS = 8
KEY_VALUE_HEADS = 2
GRID = 64
eps = 1e-06
rotary_base = 10000.0


def apply_rotary(vectors, grid_positions):
    half_size = vectors.shape[-1] // 2
    frequency = rotary_base ** (-jnp.arange(0, half_size, 2, dtype=jnp.float32) / half_size)
    grid_row = (grid_positions // GRID).astype(jnp.float32)
    grid_col = (grid_positions % GRID).astype(jnp.float32)
    angles = jnp.concatenate(
        [grid_row[:, None] * frequency, grid_col[:, None] * frequency], axis=-1
    )[:, None, :]
    cosine_table = jnp.cos(angles)
    sine_table = jnp.sin(angles)
    first_half = vectors[..., :half_size]
    second_half = vectors[..., half_size:]
    return jnp.concatenate(
        [
            first_half * cosine_table - second_half * sine_table,
            first_half * sine_table + second_half * cosine_table,
        ],
        axis=-1,
    )


def per_head_norm(vectors, gain):
    return vectors * lax.rsqrt(jnp.mean(vectors * vectors, axis=-1, keepdims=True) + eps) * gain


def on_device(
    residual_in,
    queries,
    keys,
    values,
    query_gain,
    key_norm_gain,
    out_weight,
    mlp_gain,
    gate_weight,
    up_weight,
    down_weight,
):
    local_rows = residual_in.shape[0]
    local_heads = queries.shape[1] // HEAD_SIZE
    queries_per_group = QUERY_HEADS // KEY_VALUE_HEADS
    tp_index = lax.axis_index("tp")
    grid_positions = lax.axis_index("sp") * local_rows + jnp.arange(local_rows, dtype=jnp.int32)
    query_rows = apply_rotary(
        per_head_norm(
            queries.astype(jnp.float32).reshape(local_rows, local_heads, HEAD_SIZE), query_gain
        ),
        grid_positions,
    ).astype(jnp.bfloat16)
    query_matrix = jnp.transpose(query_rows, (1, 0, 2)).reshape(local_heads * local_rows, HEAD_SIZE)
    shared = tp_index * local_heads // queries_per_group
    own_keys = lax.dynamic_slice_in_dim(keys, shared * HEAD_SIZE, HEAD_SIZE, 1)
    own_values = lax.dynamic_slice_in_dim(values, shared * HEAD_SIZE, HEAD_SIZE, 1)
    key_matrix = apply_rotary(
        per_head_norm(own_keys.astype(jnp.float32)[:, None, :], key_norm_gain), grid_positions
    )[:, 0, :].astype(jnp.bfloat16)
    score_scale = HEAD_SIZE ** (-0.5)
    query_count = local_heads * local_rows
    start_state = (
        jnp.full((query_count,), -1e30, jnp.float32),
        jnp.zeros((query_count,), jnp.float32),
        jnp.zeros((query_count, HEAD_SIZE), jnp.float32),
    )
    key_piece = lax.all_gather(key_matrix, "sp", axis=0, tiled=True)
    value_piece = lax.all_gather(own_values, "sp", axis=0, tiled=True)
    piece_rows = key_piece.shape[0]
    block_count = -(-piece_rows // 2048)
    while piece_rows % block_count:
        block_count += 1
    block_width = piece_rows // block_count

    def one_block(block_index, state_inner):
        running_max, running_sum, weighted = state_inner
        block_keys = lax.dynamic_slice_in_dim(key_piece, block_index * block_width, block_width, 0)
        block_values = lax.dynamic_slice_in_dim(
            value_piece, block_index * block_width, block_width, 0
        )
        scores = (
            jnp.dot(query_matrix, block_keys.T, preferred_element_type=jnp.float32) * score_scale
        )
        new_max = jnp.maximum(running_max, jnp.max(scores, axis=1))
        factor = jnp.exp(running_max - new_max)
        weights = jnp.exp(scores - new_max[:, None])
        running_sum = running_sum * factor + jnp.sum(weights, axis=1)
        weighted = weighted * factor[:, None] + jnp.dot(
            weights.astype(jnp.bfloat16), block_values, preferred_element_type=jnp.float32
        )
        return (new_max, running_sum, weighted)

    running_max, running_sum, weighted = lax.fori_loop(0, block_count, one_block, start_state)
    attended = (weighted / running_sum[:, None]).astype(jnp.bfloat16)
    attended = jnp.transpose(
        attended.reshape(local_heads, local_rows, HEAD_SIZE), (1, 0, 2)
    ).reshape(local_rows, local_heads * HEAD_SIZE)
    own_width = residual_in.shape[1]
    projected = jnp.dot(attended, out_weight, preferred_element_type=jnp.float32).astype(
        jnp.bfloat16
    )
    share = lax.psum_scatter(projected, "tp", scatter_dimension=1, tiled=True).astype(jnp.float32)
    residual_mid = residual_in.astype(jnp.float32) + share
    squares = lax.psum(jnp.sum(residual_mid * residual_mid, axis=1), "tp")
    gain_own = lax.dynamic_slice_in_dim(mlp_gain, tp_index * own_width, own_width, 0)
    normed_own = (residual_mid * lax.rsqrt(squares / D + eps)[:, None] * gain_own).astype(
        jnp.bfloat16
    )
    normed = lax.all_gather(normed_own, "tp", axis=1, tiled=True)
    gate_out = jnp.dot(
        normed,
        lax.all_gather(gate_weight, "sp", axis=0, tiled=True),
        preferred_element_type=jnp.float32,
    )
    up_out = jnp.dot(
        normed,
        lax.all_gather(up_weight, "sp", axis=0, tiled=True),
        preferred_element_type=jnp.float32,
    )
    hidden = (jax.nn.silu(gate_out) * up_out).astype(jnp.bfloat16)
    down_terms = jnp.dot(
        hidden,
        lax.all_gather(down_weight, "sp", axis=1, tiled=True),
        preferred_element_type=jnp.float32,
    )
    down_share = lax.psum_scatter(
        down_terms.astype(jnp.bfloat16), "tp", scatter_dimension=1, tiled=True
    ).astype(jnp.float32)
    return (residual_mid + 0.5 * down_share).astype(jnp.bfloat16)


def solution(mesh):
    in_specs = (
        P("sp", "tp"),
        P("sp", "tp"),
        P("sp", None),
        P("sp", None),
        P(),
        P(),
        P("tp", None),
        P(),
        P("sp", "tp"),
        P("sp", "tp"),
        P("tp", "sp"),
    )
    out_specs = P("sp", "tp")
    return jax.shard_map(
        on_device, mesh=mesh, in_specs=in_specs, out_specs=out_specs, check_vma=False
    )
```

profile of v0, /device:TPU:0, one launch (start us, length us, event | category | flops | bytes accessed | tf_op | source)
XLA Modules:
  0.0 573.1 jit_solution(10254005252952721331)
XLA Ops:
  6.5 0.0 copy-start
  6.6 1.2 fusion.14
  7.8 1.1 fusion.16
  9.0 0.3 broadcast_multiply_fusion.1
  9.2 0.0 copy-start.5
  9.2 1.8 subtract_convert_fusion.1
  11.1 0.8 pad_maximum_fusion.2
  11.9 0.0 all-gather.18.cloned.1.call-update
  11.9 0.0 all-gather.8.cloned.1.call-start
  11.9 0.7 constant_dynamic-slice_fusion
  12.7 0.0 all-gather.8.cloned.1.call-update
  12.7 0.0 reduce-scatter.3.cloned.1.call-start
  12.8 1.4 reshape.236
  14.1 1.7 fusion.18
  15.8 0.9 multiply_reduce_fusion.2
  16.7 0.1 add_rsqrt_fusion
  16.8 1.0 multiply_multiply_fusion
  17.8 1.4 subtract_convert_fusion
  19.2 1.1 maximum_bitcast_fusion
  20.3 0.1 copy.20
  20.3 38.6 %all-gather.18.cloned.1.call-done = bf16[6144,1,128]{2,0,1:T(8,128)(2,1)} async-done(((bf16[768,1,128]{2,0,1:T(8,128)(2,1)}), bf16[6144,1,128]{2,0,1:T(8,128)(2,1)}) %all-gather.18.cloned.1.call-update) | async-done | bytes 1572880 | tf_op jit(solution)/shard_map/all_gather | solution.py:78
  58.9 44.8 %all-gather.8.cloned.1.call-done = bf16[6144,128]{1,0:T(8,128)(2,1)} async-done(((bf16[768,128]{1,0:T(8,128)(2,1)}), bf16[6144,128]{1,0:T(8,128)(2,1)}) %all-gather.8.cloned.1.call-update) | async-done | bytes 1572880 | tf_op jit(solution)/shard_map/all_gather | solution.py:79
  103.7 57.6 %while.18 = (s32[]{:T(128)}, f32[1536]{0:T(1024)S(1)}, f32[1536]{0:T(1024)S(1)}, f32[1536,128]{1,0:T(8,128)S(1)}, bf16[6144,128]{1,0:T(8,128)(2,1)}, /*index=5*/...) while((s32[]{:T(128)}, f32[1536]{0:T(1024)S(1)}, ...), condition=%wide.region_5.6_spmd.clone, body=%wide.region_2.5_spmd.clone.sunk | while | flops 1636376064 | bytes 91193544 | solution.py:104
  103.7 7.4 %multiply_reduce_fusion.4 = (f32[1536]{0:T(1024)S(1)}, f32[2048,1536]{1,0:T(8,128)}) fusion(bf16[1536,128]{1,0:T(8,128)(2,1)S(1)} %get-tuple-element.266, bf16[6144,128]{1,0:T(8,128)(2,1)} %get-tuple-element.265, s32[]{:T(128)S(6)} %select_n.55), kind=kOutput, calls=%fused_computation.1.clone.1 | convolution fusion | flops 811596288 | bytes 13506564 | tf_op jit(solution)/shard_map/while/body/eval_jaxpr/dot_general | solution.py:93
  111.1 6.8 %fusion.49 = f32[1536]{0:T(1024)S(1)} fusion(f32[2048,1536]{1,0:T(8,128)} %get-tuple-element.236, f32[1536]{0:T(1024)S(1)} %select_maximum_fusion.2), kind=kLoop, calls=%fused_computation.3.clone.1 | loop fusion | flops 9435648 | bytes 12595200 | tf_op jit(solution)/shard_map/while/body/eval_jaxpr/reduce_sum | solution.py:98
  117.9 1.3 copy-done.1
  119.2 3.6 fusion.51
  122.9 7.4 %multiply_reduce_fusion.4 = (f32[1536]{0:T(1024)S(1)}, f32[2048,1536]{1,0:T(8,128)}) fusion(bf16[1536,128]{1,0:T(8,128)(2,1)S(1)} %get-tuple-element.266, bf16[6144,128]{1,0:T(8,128)(2,1)} %get-tuple-element.265, s32[]{:T(128)S(6)} %select_n.55), kind=kOutput, calls=%fused_computation.1.clone.1 | convolution fusion | flops 811596288 | bytes 13506564 | tf_op jit(solution)/shard_map/while/body/eval_jaxpr/dot_general | solution.py:93
  130.3 6.8 %fusion.49 = f32[1536]{0:T(1024)S(1)} fusion(f32[2048,1536]{1,0:T(8,128)} %get-tuple-element.236, f32[1536]{0:T(1024)S(1)} %select_maximum_fusion.2), kind=kLoop, calls=%fused_computation.3.clone.1 | loop fusion | flops 9435648 | bytes 12595200 | tf_op jit(solution)/shard_map/while/body/eval_jaxpr/reduce_sum | solution.py:98
  137.1 1.3 copy-done.1
  138.4 3.6 fusion.51
  142.1 7.4 %multiply_reduce_fusion.4 = (f32[1536]{0:T(1024)S(1)}, f32[2048,1536]{1,0:T(8,128)}) fusion(bf16[1536,128]{1,0:T(8,128)(2,1)S(1)} %get-tuple-element.266, bf16[6144,128]{1,0:T(8,128)(2,1)} %get-tuple-element.265, s32[]{:T(128)S(6)} %select_n.55), kind=kOutput, calls=%fused_computation.1.clone.1 | convolution fusion | flops 811596288 | bytes 13506564 | tf_op jit(solution)/shard_map/while/body/eval_jaxpr/dot_general | solution.py:93
  149.5 6.8 %fusion.49 = f32[1536]{0:T(1024)S(1)} fusion(f32[2048,1536]{1,0:T(8,128)} %get-tuple-element.236, f32[1536]{0:T(1024)S(1)} %select_maximum_fusion.2), kind=kLoop, calls=%fused_computation.3.clone.1 | loop fusion | flops 9435648 | bytes 12595200 | tf_op jit(solution)/shard_map/while/body/eval_jaxpr/reduce_sum | solution.py:98
  156.3 1.3 copy-done.1
  157.6 3.6 fusion.51
  161.3 0.3 divide_convert_fusion
  161.6 0.2 copy.21
  161.8 0.0 copy-start.2
  161.8 2.7 convolution_convert_fusion
  164.5 0.0 reduce-scatter.3.cloned.1.call-update
  164.5 0.0 all-gather.12.cloned.1.call-start
  164.6 0.5 all-gather.12.cloned.1.call-update
  165.1 0.2 all-gather.10.cloned.1.call-start
  165.3 0.8 dynamic_slice.25
  166.1 34.7 %reduce-scatter.3.cloned.1.call-done = bf16[768,512]{1,0:T(8,128)(2,1)} async-done(((bf16[768,2048]{1,0:T(8,128)(2,1)}), bf16[768,512]{1,0:T(8,128)(2,1)}) %reduce-scatter.3.cloned.1.call-update) | async-done | bytes 786448 | tf_op jit(solution)/shard_map/reduce_scatter | solution.py:113
  200.8 1.5 multiply_reduce_fusion.1
  202.2 5.8 %psum.7 = f32[768]{0:T(1024)S(1)} all-reduce(f32[768]{0:T(1024)S(1)} %multiply_reduce_fusion.1), channel_id=1, replica_groups=mesh['sp'=8,'tp'=4] {'tp'}, use_global_device_ids=true, to_apply=%region_8.9 | all-reduce | flops 768 | bytes 6144 | tf_op jit(solution)/shard_map/psum | solution.py:115
  208.0 2.3 multiply_convert_fusion.1
  210.3 0.0 all-gather.10.cloned.1.call-update
  210.3 0.0 all-gather.14.cloned.1.call-start
  210.4 0.5 all-gather.14.cloned.1.call-update
  210.9 0.0 all-gather.16.cloned.1.call-start
  211.0 0.7 all-gather.16.cloned.1.call-update
  211.7 0.0 reduce-scatter.5.cloned.1.call-start
  211.7 83.4 %all-gather.12.cloned.1.call-done = bf16[2048,1408]{1,0:T(8,128)(2,1)} async-done(((bf16[256,1408]{1,0:T(8,128)(2,1)}), bf16[2048,1408]{1,0:T(8,128)(2,1)}) %all-gather.12.cloned.1.call-update) | async-done | bytes 5767184 | tf_op jit(solution)/shard_map/all_gather | solution.py:123
  295.1 28.1 %all-gather.10.cloned.1.call-done = bf16[768,2048]{1,0:T(8,128)(2,1)} async-done(((bf16[768,512]{1,0:T(8,128)(2,1)}), bf16[768,2048]{1,0:T(8,128)(2,1)}) %all-gather.10.cloned.1.call-update) | async-done | bytes 3145744 | tf_op jit(solution)/shard_map/all_gather | solution.py:120
  323.3 9.7 %fusion.31 = f32[768,1408]{1,0:T(8,128)} fusion(bf16[768,2048]{1,0:T(8,128)(2,1)} %all-gather.10.cloned.1.call-done, bf16[2048,1408]{1,0:T(8,128)(2,1)} %all-gather.12.cloned.1.call-done), kind=kOutput, calls=%fused_computation.68 | convolution fusion | flops 4429185024 | bytes 13238272 | tf_op jit(solution)/shard_map/dot_general | solution.py:121
  333.0 84.7 %all-gather.14.cloned.1.call-done = bf16[2048,1408]{1,0:T(8,128)(2,1)} async-done(((bf16[256,1408]{1,0:T(8,128)(2,1)}), bf16[2048,1408]{1,0:T(8,128)(2,1)}) %all-gather.14.cloned.1.call-update) | async-done | bytes 5767184 | tf_op jit(solution)/shard_map/all_gather | solution.py:128
  417.6 93.4 %all-gather.16.cloned.1.call-done = bf16[1408,2048]{1,0:T(8,128)(2,1)} async-done(((bf16[1408,256]{1,0:T(8,128)(2,1)}), bf16[1408,2048]{1,0:T(8,128)(2,1)}) %all-gather.16.cloned.1.call-update) | async-done | bytes 5767184 | tf_op jit(solution)/shard_map/all_gather | solution.py:134
  511.0 16.8 %convolution_convert_fusion.1 = bf16[768,2048]{1,0:T(8,128)(2,1)} fusion(bf16[1408,2048]{1,0:T(8,128)(2,1)} %all-gather.16.cloned.1.call-done, f32[768,1408]{1,0:T(8,128)} %fusion.31, bf16[768,2048]{1,0:T(8,128)(2,1)} %all-gather.10.cloned.1.call-done, bf16[2048,1408]{1,0:T(8,128)(2,1)} %all-gather.14.cloned.1.call-done), kind=kOutput, calls=%fused_computation.19 | convolution fusion | flops 8866430976 | bytes 22151168 | tf_op jit(solution)/shard_map/dot_general | solution.py:132
  527.8 0.0 reduce-scatter.5.cloned.1.call-update
  527.8 36.1 %reduce-scatter.5.cloned.1.call-done = bf16[768,512]{1,0:T(8,128)(2,1)} async-done(((bf16[768,2048]{1,0:T(8,128)(2,1)}), bf16[768,512]{1,0:T(8,128)(2,1)}) %reduce-scatter.5.cloned.1.call-update) | async-done | bytes 786448 | tf_op jit(solution)/shard_map/reduce_scatter | solution.py:137
  563.9 0.0 copy-done.3
  563.9 2.3 add_convert_fusion
  (26 shorter events, 0.1 us)
Async XLA Ops:
  6.5 155.2 %copy-start = (bf16[256,2048]{1,0:T(8,128)(2,1)S(1)}, bf16[256,2048]{1,0:T(8,128)(2,1)}, u32[]{:S(2)}) copy-start(bf16[256,2048]{1,0:T(8,128)(2,1)} %param.19) | copy-start | bytes 3145732
  6.5 5.4 copy-start.4
  6.5 52.4 %all-gather.18.cloned.1.call-start = ((), (), s32[]{:S(2)}) async-start(), calls=%async_computation.9 | async-start | bytes 1769472 | tf_op jit(solution)/shard_map/all_gather | solution.py:78
  9.2 7.5 %copy-start.5 = (f32[128]{0:T(128)S(1)}, f32[128]{0:T(128)}, u32[]{:S(2)}) copy-start(f32[128]{0:T(128)} %param.17) | copy-start | bytes 1540
  11.9 91.8 %all-gather.8.cloned.1.call-start = ((), (), s32[]{:S(2)}) async-start(), calls=%async_computation.2 | async-start | bytes 1769472 | tf_op jit(solution)/shard_map/all_gather | solution.py:79
  12.7 188.1 %reduce-scatter.3.cloned.1.call-start = ((), (), s32[]{:S(2)}) async-start(), calls=%async_computation.3 | async-start | bytes 3932160 | tf_op jit(solution)/shard_map/reduce_scatter | solution.py:113
  111.1 8.2 %copy-start.1 = (f32[2048,1536]{1,0:T(8,128)S(1)}, f32[2048,1536]{1,0:T(8,128)}, u32[]{:S(2)}) copy-start(f32[2048,1536]{1,0:T(8,128)} %get-tuple-element.236) | copy-start | bytes 37748740 | tf_op jit(solution)/shard_map/while
  130.3 8.2 %copy-start.1 = (f32[2048,1536]{1,0:T(8,128)S(1)}, f32[2048,1536]{1,0:T(8,128)}, u32[]{:S(2)}) copy-start(f32[2048,1536]{1,0:T(8,128)} %get-tuple-element.236) | copy-start | bytes 37748740 | tf_op jit(solution)/shard_map/while
  149.5 8.2 %copy-start.1 = (f32[2048,1536]{1,0:T(8,128)S(1)}, f32[2048,1536]{1,0:T(8,128)}, u32[]{:S(2)}) copy-start(f32[2048,1536]{1,0:T(8,128)} %get-tuple-element.236) | copy-start | bytes 37748740 | tf_op jit(solution)/shard_map/while
  161.8 39.0 %copy-start.2 = (bf16[768,512]{1,0:T(8,128)(2,1)S(1)}, bf16[768,512]{1,0:T(8,128)(2,1)}, u32[]{:S(2)}) copy-start(bf16[768,512]{1,0:T(8,128)(2,1)} %param.13) | copy-start | bytes 2359300
  164.5 130.6 %all-gather.12.cloned.1.call-start = ((), (), s32[]{:S(2)}) async-start(), calls=%async_computation.5 | async-start | bytes 6488064 | tf_op jit(solution)/shard_map/all_gather | solution.py:123
  165.1 158.2 %all-gather.10.cloned.1.call-start = ((), (), s32[]{:S(2)}) async-start(), calls=%async_computation.4 | async-start | bytes 3932160 | tf_op jit(solution)/shard_map/all_gather | solution.py:120
  210.3 207.3 %all-gather.14.cloned.1.call-start = ((), (), s32[]{:S(2)}) async-start(), calls=%async_computation.6 | async-start | bytes 6488064 | tf_op jit(solution)/shard_map/all_gather | solution.py:128
  210.9 300.1 %all-gather.16.cloned.1.call-start = ((), (), s32[]{:S(2)}) async-start(), calls=%async_computation.7 | async-start | bytes 6488064 | tf_op jit(solution)/shard_map/all_gather | solution.py:134
  211.7 352.2 %reduce-scatter.5.cloned.1.call-start = ((), (), s32[]{:S(2)}) async-start(), calls=%async_computation.8 | async-start | bytes 3932160 | tf_op jit(solution)/shard_map/reduce_scatter | solution.py:137
  333.0 230.9 %copy-start.3 = (bf16[768,512]{1,0:T(8,128)(2,1)S(1)}, bf16[768,512]{1,0:T(8,128)(2,1)}, u32[]{:S(2)}) copy-start(bf16[768,512]{1,0:T(8,128)(2,1)} %reduce-scatter.3.cloned.1.call-done) | copy-start | bytes 2359300
Sparse Core Ops, SparseCore 0:
  12.0 46.8 all-gather.17
  61.1 42.5 all-gather.7
  164.6 36.0 reduce-scatter.2
  202.8 92.2 all-gather.11
  296.5 26.6 all-gather.9
  325.3 92.3 all-gather.13
  419.7 91.2 all-gather.15
  527.9 35.8 reduce-scatter.4
where the time goes:
time: 574 us; the launch traced here: 573 us
  waiting for transfers between devices  446 us (78%)
  matrix products  62.2 us (11%)
  other arithmetic  38.3 us (7%)
  between operations  13.7 us (2%)
  local copies, waits for them, and re-layouts  7.03 us (1%)
  blocking collectives  5.77 us (1%)
    all_gather x1, waiting for transfers between devices, on_device(): lax.all_gather(down_weight, 'sp', axis=1, tiled=True)  93.4 us
    all_gather x1, waiting for transfers between devices, on_device(): lax.all_gather(up_weight, 'sp', axis=0, tiled=True)  84.7 us
    all_gather x1, waiting for transfers between devices, on_device(): lax.all_gather(gate_weight, 'sp', axis=0, tiled=True)  83.4 us
    all_gather x1, waiting for transfers between devices, on_device(): value_piece = lax.all_gather(own_values, 'sp', axis=0, tiled=True)  44.8 us
    all_gather x1, waiting for transfers between devices, on_device(): key_piece = lax.all_gather(key_matrix, 'sp', axis=0, tiled=True)  38.6 us
    reduce_scatter x1, waiting for transfers between devices, on_device(): lax.psum_scatter(down_terms.astype(jnp.bfloat16), 'tp', scatter_dimension...  36.1 us
    reduce_scatter x1, waiting for transfers between devices, on_device(): lax.psum_scatter(projected, 'tp', scatter_dimension=1, tiled=True)  34.7 us
    all_gather x1, waiting for transfers between devices, on_device(): normed = lax.all_gather(normed_own, 'tp', axis=1, tiled=True)  28.1 us
  transfers between devices with their start and end apart: 8, of which 8 were waited for; matrix products, arithmetic and copies ran while one was open for 4% of the time, Pallas kernels for 0%

commit v1 on v0

--- a/solution.py
+++ b/solution.py
@@ -129,10 +129,11 @@
         preferred_element_type=jnp.float32,
     )
     hidden = (jax.nn.silu(gate_out) * up_out).astype(jnp.bfloat16)
+    read_sectors = lambda xx, axis_name: jnp.concatenate(
+        lax.all_gather(xx, axis_name=axis_name), axis=1
+    )
     down_terms = jnp.dot(
-        hidden,
-        lax.all_gather(down_weight, "sp", axis=1, tiled=True),
-        preferred_element_type=jnp.float32,
+        hidden, read_sectors(down_weight, "sp"), preferred_element_type=jnp.float32
     )
     down_share = lax.psum_scatter(
         down_terms.astype(jnp.bfloat16), "tp", scatter_dimension=1, tiled=True

time: 574 us -> 573 us (level)
  waiting for transfers between devices: 446 us -> 437 us
  local copies, waits for them, and re-layouts: 7.03 us -> 15.3 us
    all_gather x1, waiting for transfers between devices: 93.4 us -> 84 us  [on_device(): lax.all_gather(xx, axis_name=axis_name)]
    reshape x0 -> x1, local copies, waits for them, and re-layouts: none -> 8.26 us  [on_device(): jnp.concatenate(lax.all_gather(xx, axis_name=axis_name), axis=1)]
  transfers between devices with their start and end apart: 8 -> 8, of which waited for: 8 -> 8; matrix products, arithmetic and copies ran while one was open for 4% -> 5% of each run, Pallas kernels for 0% -> 0%
where the time goes in v1:
time: 573 us; the launch traced here: 572 us
  waiting for transfers between devices  437 us (76%)
  matrix products  62.2 us (11%)
  other arithmetic  38.3 us (7%)
  local copies, waits for them, and re-layouts  15.3 us (3%)
  between operations  13.7 us (2%)
  blocking collectives  5.77 us (1%)
    all_gather x1, waiting for transfers between devices, on_device(): lax.all_gather(up_weight, 'sp', axis=0, tiled=True)  84.8 us
    all_gather x1, waiting for transfers between devices, on_device(): lax.all_gather(gate_weight, 'sp', axis=0, tiled=True)  84.3 us
    all_gather x1, waiting for transfers between devices, on_device(): lax.all_gather(xx, axis_name=axis_name)  84 us
    all_gather x1, waiting for transfers between devices, on_device(): value_piece = lax.all_gather(own_values, 'sp', axis=0, tiled=True)  44.8 us
    all_gather x1, waiting for transfers between devices, on_device(): key_piece = lax.all_gather(key_matrix, 'sp', axis=0, tiled=True)  38.6 us
    reduce_scatter x1, waiting for transfers between devices, on_device(): lax.psum_scatter(down_terms.astype(jnp.bfloat16), 'tp', scatter_dimension...  36.1 us
    reduce_scatter x1, waiting for transfers between devices, on_device(): lax.psum_scatter(projected, 'tp', scatter_dimension=1, tiled=True)  34.1 us
    all_gather x1, waiting for transfers between devices, on_device(): normed = lax.all_gather(normed_own, 'tp', axis=1, tiled=True)  28.1 us
  transfers between devices with their start and end apart: 8, of which 8 were waited for; matrix products, arithmetic and copies ran while one was open for 5% of the time, Pallas kernels for 0%

profile of v1, /device:TPU:0, one launch (start us, length us, event | category | flops | bytes accessed | tf_op | source)
XLA Modules:
  0.0 572.4 jit_solution(17925022155336443010)
XLA Ops:
  6.5 0.0 copy-start
  6.6 1.2 fusion.14
  7.8 1.1 fusion.16
  9.0 0.3 broadcast_multiply_fusion.1
  9.2 0.0 copy-start.5
  9.2 1.8 subtract_convert_fusion.1
  11.1 0.8 pad_maximum_fusion.2
  11.9 0.0 all-gather.17.cloned.1.call-update
  11.9 0.0 all-gather.9.cloned.1.call-start
  11.9 0.7 constant_dynamic-slice_fusion
  12.7 0.0 all-gather.9.cloned.1.call-update
  12.7 0.0 reduce-scatter.3.cloned.1.call-start
  12.8 1.4 reshape.244
  14.1 1.7 fusion.18
  15.8 0.9 multiply_reduce_fusion.2
  16.7 0.1 add_rsqrt_fusion
  16.8 1.0 multiply_multiply_fusion
  17.8 1.4 subtract_convert_fusion
  19.2 1.1 maximum_bitcast_fusion
  20.3 0.1 copy.22
  20.3 38.6 %all-gather.17.cloned.1.call-done = bf16[6144,1,128]{2,0,1:T(8,128)(2,1)} async-done(((bf16[768,1,128]{2,0,1:T(8,128)(2,1)}), bf16[6144,1,128]{2,0,1:T(8,128)(2,1)}) %all-gather.17.cloned.1.call-update) | async-done | bytes 1572880 | tf_op jit(solution)/shard_map/all_gather | solution.py:78
  58.9 44.8 %all-gather.9.cloned.1.call-done = bf16[6144,128]{1,0:T(8,128)(2,1)} async-done(((bf16[768,128]{1,0:T(8,128)(2,1)}), bf16[6144,128]{1,0:T(8,128)(2,1)}) %all-gather.9.cloned.1.call-update) | async-done | bytes 1572880 | tf_op jit(solution)/shard_map/all_gather | solution.py:79
  103.7 57.6 %while.18 = (s32[]{:T(128)}, f32[1536]{0:T(1024)S(1)}, f32[1536]{0:T(1024)S(1)}, f32[1536,128]{1,0:T(8,128)S(1)}, bf16[6144,128]{1,0:T(8,128)(2,1)}, /*index=5*/...) while((s32[]{:T(128)}, f32[1536]{0:T(1024)S(1)}, ...), condition=%wide.region_5.6_spmd.clone, body=%wide.region_2.5_spmd.clone.sunk | while | flops 1636376064 | bytes 91193544 | solution.py:104
  103.7 7.4 %multiply_reduce_fusion.4 = (f32[1536]{0:T(1024)S(1)}, f32[2048,1536]{1,0:T(8,128)}) fusion(bf16[1536,128]{1,0:T(8,128)(2,1)S(1)} %get-tuple-element.266, bf16[6144,128]{1,0:T(8,128)(2,1)} %get-tuple-element.265, s32[]{:T(128)S(6)} %select_n.55), kind=kOutput, calls=%fused_computation.1.clone.1 | convolution fusion | flops 811596288 | bytes 13506564 | tf_op jit(solution)/shard_map/while/body/eval_jaxpr/dot_general | solution.py:93
  111.1 6.8 %fusion.49 = f32[1536]{0:T(1024)S(1)} fusion(f32[2048,1536]{1,0:T(8,128)} %get-tuple-element.236, f32[1536]{0:T(1024)S(1)} %select_maximum_fusion.2), kind=kLoop, calls=%fused_computation.3.clone.1 | loop fusion | flops 9435648 | bytes 12595200 | tf_op jit(solution)/shard_map/while/body/eval_jaxpr/reduce_sum | solution.py:98
  117.9 1.3 copy-done.1
  119.2 3.6 fusion.51
  122.9 7.4 %multiply_reduce_fusion.4 = (f32[1536]{0:T(1024)S(1)}, f32[2048,1536]{1,0:T(8,128)}) fusion(bf16[1536,128]{1,0:T(8,128)(2,1)S(1)} %get-tuple-element.266, bf16[6144,128]{1,0:T(8,128)(2,1)} %get-tuple-element.265, s32[]{:T(128)S(6)} %select_n.55), kind=kOutput, calls=%fused_computation.1.clone.1 | convolution fusion | flops 811596288 | bytes 13506564 | tf_op jit(solution)/shard_map/while/body/eval_jaxpr/dot_general | solution.py:93
  130.3 6.8 %fusion.49 = f32[1536]{0:T(1024)S(1)} fusion(f32[2048,1536]{1,0:T(8,128)} %get-tuple-element.236, f32[1536]{0:T(1024)S(1)} %select_maximum_fusion.2), kind=kLoop, calls=%fused_computation.3.clone.1 | loop fusion | flops 9435648 | bytes 12595200 | tf_op jit(solution)/shard_map/while/body/eval_jaxpr/reduce_sum | solution.py:98
  137.1 1.3 copy-done.1
  138.4 3.6 fusion.51
  142.1 7.4 %multiply_reduce_fusion.4 = (f32[1536]{0:T(1024)S(1)}, f32[2048,1536]{1,0:T(8,128)}) fusion(bf16[1536,128]{1,0:T(8,128)(2,1)S(1)} %get-tuple-element.266, bf16[6144,128]{1,0:T(8,128)(2,1)} %get-tuple-element.265, s32[]{:T(128)S(6)} %select_n.55), kind=kOutput, calls=%fused_computation.1.clone.1 | convolution fusion | flops 811596288 | bytes 13506564 | tf_op jit(solution)/shard_map/while/body/eval_jaxpr/dot_general | solution.py:93
  149.5 6.8 %fusion.49 = f32[1536]{0:T(1024)S(1)} fusion(f32[2048,1536]{1,0:T(8,128)} %get-tuple-element.236, f32[1536]{0:T(1024)S(1)} %select_maximum_fusion.2), kind=kLoop, calls=%fused_computation.3.clone.1 | loop fusion | flops 9435648 | bytes 12595200 | tf_op jit(solution)/shard_map/while/body/eval_jaxpr/reduce_sum | solution.py:98
  156.3 1.3 copy-done.1
  157.6 3.6 fusion.51
  161.3 0.3 divide_convert_fusion
  161.6 0.2 copy.23
  161.8 0.0 copy-start.2
  161.8 2.7 convolution_convert_fusion
  164.5 0.0 reduce-scatter.3.cloned.1.call-update
  164.5 0.0 all-gather.19.cloned.1.call-start
  164.6 0.5 all-gather.19.cloned.1.call-update
  165.1 0.0 all-gather.13.cloned.1.call-start
  165.1 0.5 all-gather.13.cloned.1.call-update
  165.7 0.2 all-gather.11.cloned.1.call-start
  165.9 0.8 dynamic_slice.25
  166.7 34.1 %reduce-scatter.3.cloned.1.call-done = bf16[768,512]{1,0:T(8,128)(2,1)} async-done(((bf16[768,2048]{1,0:T(8,128)(2,1)}), bf16[768,512]{1,0:T(8,128)(2,1)}) %reduce-scatter.3.cloned.1.call-update) | async-done | bytes 786448 | tf_op jit(solution)/shard_map/reduce_scatter | solution.py:113
  200.8 1.5 multiply_reduce_fusion.1
  202.2 5.8 %psum.7 = f32[768]{0:T(1024)S(1)} all-reduce(f32[768]{0:T(1024)S(1)} %multiply_reduce_fusion.1), channel_id=1, replica_groups=mesh['sp'=8,'tp'=4] {'tp'}, use_global_device_ids=true, to_apply=%region_8.9 | all-reduce | flops 768 | bytes 6144 | tf_op jit(solution)/shard_map/psum | solution.py:115
  208.0 2.3 multiply_convert_fusion.1
  210.3 0.0 all-gather.11.cloned.1.call-update
  210.3 0.0 all-gather.15.cloned.1.call-start
  210.4 0.7 all-gather.15.cloned.1.call-update
  211.1 0.0 reduce-scatter.5.cloned.1.call-start
  211.1 84.0 %all-gather.19.cloned.1.call-done = bf16[11264,256]{1,0:T(8,128)(2,1)} async-done(((bf16[1408,256]{1,0:T(8,128)(2,1)}), bf16[11264,256]{1,0:T(8,128)(2,1)}) %all-gather.19.cloned.1.call-update) | async-done | bytes 5767184 | tf_op jit(solution)/shard_map/all_gather | solution.py:133
  295.1 8.3 %copy.24 = bf16[1408,8,256]{0,2,1:T(8,128)(2,1)} copy(bf16[1408,8,256]{2,0,1:T(8,128)(2,1)} %bitcast.29) | data formatting | bytes 11534336 | tf_op jit(solution)/shard_map/reshape | solution.py:132
  303.4 84.3 %all-gather.13.cloned.1.call-done = bf16[2048,1408]{1,0:T(8,128)(2,1)} async-done(((bf16[256,1408]{1,0:T(8,128)(2,1)}), bf16[2048,1408]{1,0:T(8,128)(2,1)}) %all-gather.13.cloned.1.call-update) | async-done | bytes 5767184 | tf_op jit(solution)/shard_map/all_gather | solution.py:123
  387.7 28.1 %all-gather.11.cloned.1.call-done = bf16[768,2048]{1,0:T(8,128)(2,1)} async-done(((bf16[768,512]{1,0:T(8,128)(2,1)}), bf16[768,2048]{1,0:T(8,128)(2,1)}) %all-gather.11.cloned.1.call-update) | async-done | bytes 3145744 | tf_op jit(solution)/shard_map/all_gather | solution.py:120
  415.8 9.7 %fusion.31 = f32[768,1408]{1,0:T(8,128)} fusion(bf16[768,2048]{1,0:T(8,128)(2,1)} %all-gather.11.cloned.1.call-done, bf16[2048,1408]{1,0:T(8,128)(2,1)} %all-gather.13.cloned.1.call-done), kind=kOutput, calls=%fused_computation.68 | convolution fusion | flops 4429185024 | bytes 13238272 | tf_op jit(solution)/shard_map/dot_general | solution.py:121
  425.5 84.8 %all-gather.15.cloned.1.call-done = bf16[2048,1408]{1,0:T(8,128)(2,1)} async-done(((bf16[256,1408]{1,0:T(8,128)(2,1)}), bf16[2048,1408]{1,0:T(8,128)(2,1)}) %all-gather.15.cloned.1.call-update) | async-done | bytes 5767184 | tf_op jit(solution)/shard_map/all_gather | solution.py:128
  510.4 16.8 %convolution_convert_fusion.1 = bf16[768,2048]{1,0:T(8,128)(2,1)} fusion(bf16[1408,2048]{0,1:T(8,128)(2,1)} %bitcast.30, f32[768,1408]{1,0:T(8,128)} %fusion.31, bf16[768,2048]{1,0:T(8,128)(2,1)} %all-gather.11.cloned.1.call-done, bf16[2048,1408]{1,0:T(8,128)(2,1)} %all-gather.15.cloned.1.call-done), kind=kOutput, calls=%fused_computation.19 | convolution fusion | flops 8866430976 | bytes 22151168 | tf_op jit(solution)/shard_map/dot_general | solution.py:135
  527.1 0.0 reduce-scatter.5.cloned.1.call-update
  527.2 36.1 %reduce-scatter.5.cloned.1.call-done = bf16[768,512]{1,0:T(8,128)(2,1)} async-done(((bf16[768,2048]{1,0:T(8,128)(2,1)}), bf16[768,512]{1,0:T(8,128)(2,1)}) %reduce-scatter.5.cloned.1.call-update) | async-done | bytes 786448 | tf_op jit(solution)/shard_map/reduce_scatter | solution.py:138
  563.2 2.3 add_convert_fusion
  (27 shorter events, 0.1 us)
Async XLA Ops:
  6.5 155.2 %copy-start = (bf16[256,2048]{1,0:T(8,128)(2,1)S(1)}, bf16[256,2048]{1,0:T(8,128)(2,1)}, u32[]{:S(2)}) copy-start(bf16[256,2048]{1,0:T(8,128)(2,1)} %param.19) | copy-start | bytes 3145732
  6.5 5.4 copy-start.4
  6.5 52.4 %all-gather.17.cloned.1.call-start = ((), (), s32[]{:S(2)}) async-start(), calls=%async_computation.8 | async-start | bytes 1769472 | tf_op jit(solution)/shard_map/all_gather | solution.py:78
  9.2 7.5 %copy-start.5 = (f32[128]{0:T(128)S(1)}, f32[128]{0:T(128)}, u32[]{:S(2)}) copy-start(f32[128]{0:T(128)} %param.17) | copy-start | bytes 1540
  11.9 91.8 %all-gather.9.cloned.1.call-start = ((), (), s32[]{:S(2)}) async-start(), calls=%async_computation.2 | async-start | bytes 1769472 | tf_op jit(solution)/shard_map/all_gather | solution.py:79
  12.7 188.1 %reduce-scatter.3.cloned.1.call-start = ((), (), s32[]{:S(2)}) async-start(), calls=%async_computation.3 | async-start | bytes 3932160 | tf_op jit(solution)/shard_map/reduce_scatter | solution.py:113
  111.1 8.2 %copy-start.1 = (f32[2048,1536]{1,0:T(8,128)S(1)}, f32[2048,1536]{1,0:T(8,128)}, u32[]{:S(2)}) copy-start(f32[2048,1536]{1,0:T(8,128)} %get-tuple-element.236) | copy-start | bytes 37748740 | tf_op jit(solution)/shard_map/while
  130.3 8.2 %copy-start.1 = (f32[2048,1536]{1,0:T(8,128)S(1)}, f32[2048,1536]{1,0:T(8,128)}, u32[]{:S(2)}) copy-start(f32[2048,1536]{1,0:T(8,128)} %get-tuple-element.236) | copy-start | bytes 37748740 | tf_op jit(solution)/shard_map/while
  149.5 8.2 %copy-start.1 = (f32[2048,1536]{1,0:T(8,128)S(1)}, f32[2048,1536]{1,0:T(8,128)}, u32[]{:S(2)}) copy-start(f32[2048,1536]{1,0:T(8,128)} %get-tuple-element.236) | copy-start | bytes 37748740 | tf_op jit(solution)/shard_map/while
  161.8 39.0 %copy-start.2 = (bf16[768,512]{1,0:T(8,128)(2,1)S(1)}, bf16[768,512]{1,0:T(8,128)(2,1)}, u32[]{:S(2)}) copy-start(bf16[768,512]{1,0:T(8,128)(2,1)} %param.13) | copy-start | bytes 2359300
  164.5 130.6 %all-gather.19.cloned.1.call-start = ((), (), s32[]{:S(2)}) async-start(), calls=%async_computation.9 | async-start | bytes 6488064 | tf_op jit(solution)/shard_map/all_gather | solution.py:133
  165.1 222.6 %all-gather.13.cloned.1.call-start = ((), (), s32[]{:S(2)}) async-start(), calls=%async_computation.5 | async-start | bytes 6488064 | tf_op jit(solution)/shard_map/all_gather | solution.py:123
  165.7 250.1 %all-gather.11.cloned.1.call-start = ((), (), s32[]{:S(2)}) async-start(), calls=%async_computation.4 | async-start | bytes 3932160 | tf_op jit(solution)/shard_map/all_gather | solution.py:120
  210.3 300.0 %all-gather.15.cloned.1.call-start = ((), (), s32[]{:S(2)}) async-start(), calls=%async_computation.6 | async-start | bytes 6488064 | tf_op jit(solution)/shard_map/all_gather | solution.py:128
  211.1 352.1 %reduce-scatter.5.cloned.1.call-start = ((), (), s32[]{:S(2)}) async-start(), calls=%async_computation.7 | async-start | bytes 3932160 | tf_op jit(solution)/shard_map/reduce_scatter | solution.py:138
  510.4 52.9 %copy-start.3 = (bf16[768,512]{1,0:T(8,128)(2,1)S(1)}, bf16[768,512]{1,0:T(8,128)(2,1)}, u32[]{:S(2)}) copy-start(bf16[768,512]{1,0:T(8,128)(2,1)} %reduce-scatter.3.cloned.1.call-done) | copy-start | bytes 2359300
Sparse Core Ops, SparseCore 0:
  12.0 46.8 all-gather.16
  61.1 42.5 all-gather.8
  164.6 36.0 reduce-scatter.2
  202.8 92.2 all-gather.18
  297.2 90.4 all-gather.12
  389.1 26.6 all-gather.10
  418.0 92.3 all-gather.14
  527.3 35.8 reduce-scatter.4
